TPU v7x, 32 devices: a whole 2x2x4 slice. The times are simulated.
32 devices in a mesh: ep: 8 (over z, core), tp: 4 (over y, x).
Axes of the slice: x: 2, y: 2, z: 4, core: 2. Of those that a mesh axis runs over, the one named last changes fastest.
Arguments:
- token_rows: bfloat16 [192, 2048], P('ep', 'tp'), may hold values from -6 to 6
- prior_state: float32 [192, 64, 2048], P('ep', None, 'tp'), may hold values from -4 to 4
- first_gain: bfloat16 [2048], replicated, may hold values from 0.099609375 to 1.8984375
- w_recept: bfloat16 [2048, 2048], P(None, 'tp'), may hold values from -0.125 to 0.125
- w_key: bfloat16 [2048, 2048], P(None, 'tp'), may hold values from -0.125 to 0.125
- w_value: bfloat16 [2048, 2048], P(None, 'tp'), may hold values from -0.125 to 0.125
- decay_down: bfloat16 [2048, 96], P('tp'), may hold values from -0.125 to 0.125
- decay_up: bfloat16 [96, 2048], P(None, 'tp'), may hold values from -0.625 to 0.625
- decay_base: float32 [2048], P('tp'), may hold values from -4 to 3
- iclr_down: bfloat16 [2048, 96], P('tp'), may hold values from -0.125 to 0.125
- iclr_up: bfloat16 [96, 2048], P(None, 'tp'), may hold values from -0.625 to 0.625
- iclr_base: float32 [2048], P('tp'), may hold values from -4 to 4
- key_scale: bfloat16 [2048], P('tp'), may hold values from 0.29882812 to 1.5
- key_mix: bfloat16 [2048], P('tp'), may hold values from 0 to 2
- head_gain: bfloat16 [2048], P('tp'), may hold values from 0.099609375 to 1.8984375
- w_out: bfloat16 [2048, 2048], P(None, 'tp'), may hold values from -0.125 to 0.125
- second_gain: bfloat16 [2048], replicated, may hold values from 0.099609375 to 1.8984375
- routes: int32 [192, 4], P('ep'), may hold values from 0 to 7, all different within a row; in each aligned block of 24 rows (0 to 23, 24 to 47, ...) at most 18 rows name the same one
- route_weights: float32 [192, 4], P('ep'), may hold values from 0.2 to 1
- exp_gate: bfloat16 [8, 2048, 2048], P('ep', None, 'tp'), may hold values from -0.125 to 0.125
- exp_up: bfloat16 [8, 2048, 2048], P('ep', None, 'tp'), may hold values from -0.125 to 0.125
- exp_down: bfloat16 [8, 2048, 2048], P('ep', 'tp'), may hold values from -0.125 to 0.125
- dense_gate: bfloat16 [2048, 512], P(None, 'tp'), may hold values from -0.125 to 0.125
- dense_up: bfloat16 [2048, 512], P(None, 'tp'), may hold values from -0.125 to 0.125
- dense_down: bfloat16 [512, 2048], P('tp'), may hold values from -0.25 to 0.25
- dense_mix: bfloat16 [2048], replicated, may hold values from -0.125 to 0.125
Outputs:
- layer_out: bfloat16 [192, 2048], P('ep', 'tp')
- next_state: float32 [192, 64, 2048], P('ep', None, 'tp')
Inputs may be any that keep to these rules, and one draw needn't show every extreme that they name: `routes`: each row names 4 different experts. Among the rows of one index of ep no expert is named by more than 18 rows, and in every draw some expert is named by exactly 18 of them.
All inputs are finite; a program needn't handle non-finite values.
Results may differ from a plain program's by a relative error of at most 0.018.
Values may be sent and summed in bfloat16 or wider, within the bound.
A program may use at most 64 MiB of HBM per device.

v0:
```python
import jax
import jax.numpy as jnp
from jax import lax
from jax.sharding import PartitionSpec as P

HEAD = 64
norm_eps = 1e-06
head_eps = 0.00064
key_eps = 1e-06


def product(left, right):
    return jnp.dot(left, right, preferred_element_type=jnp.float32)


def scale_rows(values, mean_square, gain):
    return (values * lax.rsqrt(mean_square + norm_eps) * gain.astype(jnp.float32)).astype(
        jnp.bfloat16
    )


def first_norm_rows(token_rows, gain):
    own_width = token_rows.shape[1]
    start = lax.axis_index("tp") * own_width
    gathered = lax.all_gather(token_rows, "tp", axis=1, tiled=True)
    values = gathered.astype(jnp.float32)
    full_rows = scale_rows(values, jnp.mean(values * values, axis=1, keepdims=True), gain)
    own_cols = lax.dynamic_slice_in_dim(full_rows, start, own_width, 1)
    return (full_rows, own_cols)


def second_norm_rows(residual, gain):
    own_width = residual.shape[1]
    start = lax.axis_index("tp") * own_width
    gathered = lax.all_gather(residual, "tp", axis=1, tiled=True)
    values = gathered.astype(jnp.float32)
    full_rows = scale_rows(values, jnp.mean(values * values, axis=1, keepdims=True), gain)
    own_cols = lax.dynamic_slice_in_dim(full_rows, start, own_width, 1)
    return (full_rows, own_cols)


def local(
    token_rows,
    prior_state,
    first_gain,
    w_recept,
    w_key,
    w_value,
    decay_down,
    decay_up,
    decay_base,
    iclr_down,
    iclr_up,
    iclr_base,
    key_scale,
    key_mix,
    head_gain,
    w_out,
    second_gain,
    routes,
    route_weights,
    exp_gate,
    exp_up,
    exp_down,
    dense_gate,
    dense_up,
    dense_down,
    dense_mix,
):
    seq_count, own_width = token_rows.shape
    heads_dev = own_width // HEAD
    first_full, first_own = first_norm_rows(token_rows, first_gain)
    decay_low, rate_low = lax.psum(
        (product(first_own, decay_down), product(first_own, iclr_down)), "tp"
    )
    decay_act = jnp.tanh(decay_low).astype(jnp.bfloat16)
    rate_act = rate_low.astype(jnp.bfloat16)
    recept = product(first_full, w_recept).astype(jnp.bfloat16)
    key_rows = product(first_full, w_key).astype(jnp.bfloat16)
    value_rows = product(first_full, w_value).astype(jnp.bfloat16)
    decay_rate = jnp.exp(
        -jnp.exp(-jax.nn.softplus(-(decay_base + product(decay_act, decay_up))) - 0.5)
    )
    iclr_rate = jax.nn.sigmoid(iclr_base + product(rate_act, iclr_up))
    key_float = key_rows.astype(jnp.float32)
    scaled = (key_float * key_scale.astype(jnp.float32)).reshape(seq_count, heads_dev, HEAD)
    removal = scaled * lax.rsqrt(jnp.sum(scaled * scaled, axis=-1, keepdims=True) + key_eps)
    written = (key_float * (1.0 + (iclr_rate - 1.0) * key_mix.astype(jnp.float32))).reshape(
        seq_count, heads_dev, HEAD
    )
    state_grid = prior_state.reshape(seq_count, HEAD, heads_dev, HEAD)
    recall = jnp.sum(state_grid * removal[:, None], axis=-1)
    scaled_removal = removal * iclr_rate.reshape(seq_count, heads_dev, HEAD)
    value_cols = jnp.transpose(
        value_rows.astype(jnp.float32).reshape(seq_count, heads_dev, HEAD), (0, 2, 1)
    )
    state_grid = (
        state_grid * decay_rate.reshape(seq_count, 1, heads_dev, HEAD)
        - recall[..., None] * scaled_removal[:, None]
        + value_cols[..., None] * written[:, None]
    )
    read = jnp.sum(
        state_grid * recept.astype(jnp.float32).reshape(seq_count, 1, heads_dev, HEAD), axis=-1
    )
    read = jnp.transpose(read, (0, 2, 1))
    centered = read - jnp.mean(read, axis=-1, keepdims=True)
    variance = jnp.mean(centered * centered, axis=-1, keepdims=True)
    head_out = (
        centered
        * lax.rsqrt(variance + head_eps)
        * head_gain.astype(jnp.float32).reshape(heads_dev, HEAD)
    )
    head_out = head_out.reshape(seq_count, own_width).astype(jnp.bfloat16)
    heads_all = lax.all_gather(head_out, "tp", axis=1, tiled=True)
    mixer_out = product(heads_all, w_out).astype(jnp.bfloat16)
    residual = (token_rows.astype(jnp.float32) + mixer_out.astype(jnp.float32)).astype(jnp.bfloat16)
    second_full, second_own = second_norm_rows(residual, second_gain)
    dense_hidden = (
        jax.nn.silu(product(second_full, dense_gate)) * product(second_full, dense_up)
    ).astype(jnp.bfloat16)
    dense_out = lax.psum_scatter(
        product(dense_hidden, dense_down).astype(jnp.bfloat16),
        "tp",
        scatter_dimension=1,
        tiled=True,
    ).astype(jnp.float32)
    mix_gate = jax.nn.sigmoid(product(second_full, dense_mix[:, None])[:, 0])
    group_count = lax.axis_size("ep")
    local_experts = exp_gate.shape[0]
    experts = local_experts * group_count
    top_count = routes.shape[1]
    capacity = max(2, 3 * seq_count * top_count // (2 * experts))
    assign_count = seq_count * top_count
    flat_ids = routes.reshape(assign_count)
    onehot = (flat_ids[:, None] == jnp.arange(experts, dtype=jnp.int32)[None, :]).astype(
        jnp.float32
    )
    earlier = (jnp.arange(assign_count)[:, None] > jnp.arange(assign_count)[None, :]).astype(
        jnp.float32
    )
    before = jnp.dot(earlier, onehot, precision=lax.Precision.HIGHEST)
    ranking = jnp.sum(before * onehot, axis=1).astype(jnp.int32)
    slot_index = flat_ids * capacity + ranking
    slot_total = experts * capacity
    slot_onehot = (jnp.arange(slot_total, dtype=jnp.int32)[:, None] == slot_index[None, :]).astype(
        jnp.bfloat16
    )
    repeated = jnp.repeat(second_full, top_count, axis=0)
    outgoing = product(slot_onehot, repeated).astype(jnp.bfloat16)
    outgoing = outgoing.reshape(group_count, local_experts, capacity, second_full.shape[1])
    arrived = lax.all_to_all(outgoing, "ep", split_axis=0, concat_axis=0, tiled=True)
    gate_act = jnp.einsum("secd,edf->secf", arrived, exp_gate, preferred_element_type=jnp.float32)
    up_act = jnp.einsum("secd,edf->secf", arrived, exp_up, preferred_element_type=jnp.float32)
    hidden = (jax.nn.silu(gate_act) * up_act).astype(jnp.bfloat16)
    partial_value = jnp.einsum(
        "secf,efd->secd", hidden, exp_down, preferred_element_type=jnp.float32
    ).astype(jnp.bfloat16)
    partial_value = lax.optimization_barrier(partial_value)
    summed = lax.psum_scatter(
        partial_value.astype(jnp.float32).astype(jnp.bfloat16),
        "tp",
        scatter_dimension=3,
        tiled=True,
    )
    returned = lax.all_to_all(summed, "ep", split_axis=0, concat_axis=0, tiled=True)
    returned = returned.reshape(slot_total, own_width)
    picked = jnp.take(returned, slot_index, axis=0).astype(jnp.float32)
    weighted = picked * route_weights.reshape(assign_count)[:, None]
    routed = jnp.sum(weighted.reshape(seq_count, top_count, own_width), axis=1)
    layer_out = residual.astype(jnp.float32) + routed + mix_gate[:, None] * dense_out
    return (layer_out.astype(jnp.bfloat16), state_grid.reshape(seq_count, HEAD, own_width))


def solution(mesh):
    in_specs = (
        P("ep", "tp"),
        P("ep", None, "tp"),
        P(),
        P(None, "tp"),
        P(None, "tp"),
        P(None, "tp"),
        P("tp", None),
        P(None, "tp"),
        P("tp"),
        P("tp", None),
        P(None, "tp"),
        P("tp"),
        P("tp"),
        P("tp"),
        P("tp"),
        P(None, "tp"),
        P(),
        P("ep", None),
        P("ep", None),
        P("ep", None, "tp"),
        P("ep", None, "tp"),
        P("ep", "tp", None),
        P(None, "tp"),
        P(None, "tp"),
        P("tp", None),
        P(),
    )
    out_specs = (P("ep", "tp"), P("ep", None, "tp"))
    return jax.shard_map(local, mesh=mesh, in_specs=in_specs, out_specs=out_specs, check_vma=False)
```

profile of v0, /device:TPU:0, one launch (start us, length us, event | category | flops | bytes accessed | tf_op | source)
XLA Modules:
  0.0 181.4 jit_solution(9681087698319180133)
XLA Ops:
  7.2 0.8 convert_element_type.135
  10.2 1.3 convert_element_type.149
  13.2 10.0 %all_gather.9 = bf16[24,2048]{1,0:T(8,128)(2,1)S(1)} all-gather(bf16[24,512]{1,0:T(8,128)(2,1)} %param.26), channel_id=1, replica_groups=mesh['ep'=8,'tp'=4] {'tp'}, dimensions={1}, use_global_device_ids=true | all-gather | bytes 122880 | tf_op jit(solution)/shard_map/all_gather | solution.py:25
  23.4 1.0 fusion.62
  24.5 1.0 fusion.64
  25.5 2.0 %fusion.29 = f32[24,512]{1,0:T(8,128)S(1)} fusion(bf16[24,2048]{1,0:T(8,128)(2,1)S(1)} %fusion.51, bf16[2048,512]{1,0:T(8,128)(2,1)} %param.29), kind=kOutput, calls=%fused_computation.30 | convolution fusion | flops 50356224 | bytes 2244608 | tf_op jit(solution)/shard_map/dot_general | solution.py:13
  27.6 2.0 %fusion.30 = f32[24,512]{1,0:T(8,128)S(1)} fusion(bf16[24,2048]{1,0:T(8,128)(2,1)S(1)} %fusion.51, bf16[2048,512]{1,0:T(8,128)(2,1)} %param.31), kind=kOutput, calls=%fused_computation.32 | convolution fusion | flops 50356224 | bytes 2244608 | tf_op jit(solution)/shard_map/dot_general | solution.py:13
  29.7 2.0 %broadcast_multiply_fusion.1 = (f32[24,512]{1,0:T(8,128)S(1)}, f32[24,512]{1,0:T(8,128)S(1)}) fusion(f32[512]{0:T(512)S(1)} %convert_element_type.135, bf16[24,2048]{1,0:T(8,128)(2,1)S(1)} %fusion.51, bf16[2048,512]{1,0:T(8,128)(2,1)} %param.30), kind=kOutput, calls=%fused_computation.81 | convolution fusion | flops 50368512 | bytes 2295808 | tf_op jit(solution)/shard_map/dot_general | solution.py:13
  32.1 15.2 %all-reduce = (bf16[24,96]{1,0:T(8,128)(2,1)S(1)}, f32[24,96]{1,0:T(8,128)S(1)}) all-reduce(f32[24,96]{1,0:T(8,128)S(1)} %fusion.62, f32[24,96]{1,0:T(8,128)S(1)} %fusion.64), channel_id=1, replica_groups=mesh['ep'=8,'tp'=4] {'tp'}, use_global_device_ids=true, to_apply=%region_4.5 | all-reduce | flops 4608 | bytes 32256 | tf_op jit(solution)/shard_map/psum | solution.py:73
  49.5 5.6 %reshape.195 = f32[24,64,8,64]{3,2,1,0:T(8,128)} reshape(f32[24,64,512]{2,1,0:T(8,128)} %param.27) | data formatting | bytes 6291456 | tf_op jit(solution)/shard_map/reshape | solution.py:91
  55.1 4.7 %multiply_reduce_fusion.1 = f32[24,64,8]{2,1,0:T(8,128)S(1)} fusion(f32[24,64,8,64]{3,2,1,0:T(8,128)} %reshape.195, f32[24,8,64]{2,1,0:T(8,128)S(1)} %get-tuple-element.5), kind=kLoop, calls=%fused_computation.2 | loop fusion | flops 1560576 | bytes 3244032 | tf_op jit(solution)/shard_map/reduce_sum | solution.py:92
  59.8 5.8 %multiply_reduce_fusion = f32[24,64,8]{2,1,0:T(8,128)S(1)} fusion(f32[24,64,8,64]{3,2,1,0:T(8,128)S(1)} %copy-done.1, f32[24,8,64]{2,1,0:T(8,128)S(1)} %reshape.208, f32[24,8,64]{2,1,0:T(8,128)S(1)} %mul.280, f32[24,64,8]{2,1,0:T(8,128)S(1)} %copy.44, f32[24,8,64]{2,1,0:T(8,128)S(1)} %get-tuple-element.4, f32[24,64,8]{2,1,0:T(8,128)S(1)} %multiply_reduce_fusion.1, ...), kind=kLoop, calls=%fused_computation.1 | loop fusion | flops 5492736 | bytes 3489792 | tf_op jit(solution)/shard_map/reduce_sum | solution.py:102
  66.3 8.4 %all_gather.10 = bf16[24,2048]{1,0:T(8,128)(2,1)S(1)} all-gather(bf16[24,512]{1,0:T(8,128)(2,1)S(1)} %convert_element_type.141), channel_id=1, replica_groups=mesh['ep'=8,'tp'=4] {'tp'}, dimensions={1}, use_global_device_ids=true | all-gather | bytes 122880 | tf_op jit(solution)/shard_map/all_gather | solution.py:114
  74.7 2.0 %fusion.28 = bf16[24,512]{1,0:T(8,128)(2,1)S(1)} fusion(bf16[24,2048]{1,0:T(8,128)(2,1)S(1)} %all_gather.10, bf16[2048,512]{1,0:T(8,128)(2,1)} %param.41, bf16[24,512]{1,0:T(8,128)(2,1)S(1)} %copy-done.12), kind=kOutput, calls=%fused_computation.28 | convolution fusion | flops 50393088 | bytes 2244608 | tf_op jit(solution)/shard_map/dot_general | solution.py:13
  76.6 7.3 %all_gather.11 = bf16[24,2048]{1,0:T(8,128)(2,1)S(1)} all-gather(bf16[24,512]{1,0:T(8,128)(2,1)S(1)} %fusion.28), channel_id=1, replica_groups=mesh['ep'=8,'tp'=4] {'tp'}, dimensions={1}, use_global_device_ids=true | all-gather | bytes 122880 | tf_op jit(solution)/shard_map/all_gather | solution.py:35
  85.0 0.8 reshape.200
  85.9 1.3 convolution_convert_fusion.1
  87.2 1.1 reshape.201
  88.2 25.8 %all_to_all.10 = bf16[8,1,18,2048]{3,2,1,0:T(8,128)(2,1)S(1)} all-to-all(bf16[8,1,18,2048]{3,2,1,0:T(8,128)(2,1)} %bitcast.112), channel_id=1, replica_groups=mesh['ep'=8,'tp'=4] {'ep'}, dimensions={0} | all-to-all | bytes 1179648 | tf_op jit(solution)/shard_map/all_to_all | solution.py:151
  114.0 0.9 copy-done.3
  114.9 2.9 %fusion.6 = f32[8,1,18,512]{3,2,0,1:T(8,128)} fusion(bf16[1,2048,512]{2,1,0:T(8,128)(2,1)} %param.45, bf16[8,1,18,2048]{3,2,1,0:T(8,128)(2,1)S(1)} %all_to_all.10), kind=kOutput, calls=%fused_computation.13 | convolution fusion | flops 301989888 | bytes 2981888 | tf_op jit(solution)/shard_map/secd,edf->secf/dot_general | solution.py:152
  117.9 3.9 %fusion = bf16[8,1,18,2048]{3,2,0,1:T(8,128)(2,1)} fusion(bf16[1,512,2048]{2,1,0:T(8,128)(2,1)S(1)} %copy-done, bf16[1,2048,512]{2,1,0:T(8,128)(2,1)} %param.46, bf16[8,1,18,2048]{3,2,1,0:T(8,128)(2,1)} %copy-done.3, f32[8,1,18,512]{3,2,0,1:T(8,128)} %fusion.6), kind=kOutput, calls=%fused_computation.6 | convolution fusion | flops 604717056 | bytes 5668864 | tf_op jit(solution)/shard_map/secf,efd->secd/dot_general | solution.py:155
  122.9 2.2 %convolution_convert_fusion.2 = bf16[24,2048]{1,0:T(8,128)(2,1)} fusion(bf16[128,2048]{1,0:T(8,128)(2,1)} %param.50, bf16[24,2048]{1,0:T(8,128)(2,1)S(1)} %copy-done.5, bf16[2048,128]{1,0:T(8,128)(2,1)} %param.49, f32[24,128]{1,0:T(8,128)} %fusion.80), kind=kOutput, calls=%fused_computation.7 | convolution fusion | flops 25233408 | bytes 1257472 | tf_op jit(solution)/shard_map/dot_general | solution.py:13
  129.1 5.3 %mul.272 = f32[24,64,8,64]{3,2,1,0:T(8,128)} broadcast(f32[24,64,8]{2,1,0:T(8,128)} %copy-done.2), dimensions={0,1,2} | broadcast | bytes 3194880 | tf_op jit(solution)/shard_map/mul | solution.py:99
  134.4 6.3 %mul.315 = f32[24,64,512]{2,1,0:T(8,128)} reshape(f32[24,64,8,64]{3,2,1,0:T(8,128)} %mul.272) | data formatting | bytes 6291456 | tf_op jit(solution)/shard_map/mul | solution.py:99
  140.7 3.8 %mul.276 = f32[24,64,8,64]{3,2,1,0:T(8,128)} broadcast(f32[24,64,8]{2,1,0:T(8,128)S(1)} %copy.44), dimensions={0,1,2} | broadcast | bytes 3194880 | tf_op jit(solution)/shard_map/mul | solution.py:100
  144.5 6.3 %mul.321 = f32[24,64,512]{2,1,0:T(8,128)} reshape(f32[24,64,8,64]{3,2,1,0:T(8,128)} %mul.276) | data formatting | bytes 6291456 | tf_op jit(solution)/shard_map/mul | solution.py:100
  150.8 7.0 %multiply_add_fusion = f32[24,64,512]{2,1,0:T(8,128)} fusion(f32[24,64,512]{2,1,0:T(8,128)} %mul.321, f32[24,64,512]{2,1,0:T(8,128)} %mul.315, f32[24,64,512]{2,1,0:T(8,128)} %param.27, f32[24,512]{1,0:T(8,128)S(1)} %get-tuple-element.7, f32[24,512]{1,0:T(8,128)S(1)} %copy-done.9, f32[24,512]{1,0:T(8,128)S(1)} %copy-done.11), kind=kLoop, calls=%fused_computation.3 | loop fusion | flops 3932160 | bytes 12730368 | tf_op jit(solution)/shard_map/add | solution.py:98
  157.8 3.4 %all-to-all-start.1 = ((bf16[8,1,18,512]{3,2,1,0:T(8,128)(2,1)}), bf16[8,1,18,512]{3,2,1,0:T(8,128)(2,1)S(1)}, u32[]{:S(2)}, u32[]{:S(2)}) async-start(bf16[8,1,18,512]{3,2,1,0:T(8,128)(2,1)} %bitcast.114), calls=%async_computation.2 | async-start | bytes 393216 | tf_op jit(solution)/shard_map/all_to_all | solution.py:165
  161.2 8.2 %all-to-all-done.1 = bf16[8,1,18,512]{3,2,1,0:T(8,128)(2,1)S(1)} async-done(((bf16[8,1,18,512]{3,2,1,0:T(8,128)(2,1)}), bf16[8,1,18,512]{3,2,1,0:T(8,128)(2,1)S(1)}, u32[]{:S(2)}, u32[]{:S(2)}) %all-to-all-start.1) | async-done | bytes 147488 | tf_op jit(solution)/shard_map/all_to_all | solution.py:165
  170.5 2.6 %reduce-scatter.5.cloned.1.call-done = bf16[24,512]{1,0:T(8,128)(2,1)} async-done(((bf16[24,2048]{1,0:T(8,128)(2,1)}), bf16[24,512]{1,0:T(8,128)(2,1)}) %reduce-scatter.5.cloned.1.call-update) | async-done | bytes 24592 | tf_op jit(solution)/shard_map/reduce_scatter | solution.py:121
  173.1 1.4 add_convert_fusion
  (98 shorter events, 14.6 us)
Async XLA Ops:
  7.2 110.7 %copy-start = (bf16[1,512,2048]{2,1,0:T(8,128)(2,1)S(1)}, bf16[1,512,2048]{2,1,0:T(8,128)(2,1)}, u32[]{:S(2)}) copy-start(bf16[1,512,2048]{2,1,0:T(8,128)(2,1)} %param.47) | copy-start | bytes 6291460
  7.2 150.6 %reduce-scatter.3.cloned.1.call-start = ((), (), s32[]{:S(2)}) async-start(), calls=%async_computation.4 | async-start | bytes 983040 | tf_op jit(solution)/shard_map/reduce_scatter | solution.py:159
  12.5 19.2 %copy-start.18 = (f32[96]{0:T(128)}, f32[96]{0:T(128)S(1)}, u32[]{:S(2)}) copy-start(f32[96]{0:T(128)S(1)} %fusion.33) | copy-start | bytes 1156
  27.5 19.9 %copy-start.13 = (bf16[96,512]{1,0:T(8,128)(2,1)S(1)}, bf16[96,512]{1,0:T(8,128)(2,1)}, u32[]{:S(2)}) copy-start(bf16[96,512]{1,0:T(8,128)(2,1)} %param.36) | copy-start | bytes 294916
  27.5 19.9 %copy-start.15 = (f32[512]{0:T(512)S(1)}, f32[512]{0:T(512)}, u32[]{:S(2)}) copy-start(f32[512]{0:T(512)} %param.37) | copy-start | bytes 6148
  27.6 20.8 %copy-start.16 = (bf16[96,512]{1,0:T(8,128)(2,1)S(1)}, bf16[96,512]{1,0:T(8,128)(2,1)}, u32[]{:S(2)}) copy-start(bf16[96,512]{1,0:T(8,128)(2,1)} %param.33) | copy-start | bytes 294916
  27.6 20.8 %copy-start.17 = (f32[512]{0:T(512)S(1)}, f32[512]{0:T(512)}, u32[]{:S(2)}) copy-start(f32[512]{0:T(512)} %param.34) | copy-start | bytes 6148
  48.6 0.6 copy-start.10
  55.1 4.7 %copy-start.1 = (f32[24,64,8,64]{3,2,1,0:T(8,128)S(1)}, f32[24,64,8,64]{3,2,1,0:T(8,128)}, u32[]{:S(2)}) copy-start(f32[24,64,8,64]{3,2,1,0:T(8,128)} %reshape.195) | copy-start | bytes 9437188
  59.8 5.8 %copy-start.2 = (f32[24,64,8]{2,1,0:T(8,128)}, f32[24,64,8]{2,1,0:T(8,128)S(1)}, u32[]{:S(2)}) copy-start(f32[24,64,8]{2,1,0:T(8,128)S(1)} %multiply_reduce_fusion.1) | copy-start | bytes 147460
  65.6 9.1 %copy-start.12 = (bf16[24,512]{1,0:T(8,128)(2,1)S(1)}, bf16[24,512]{1,0:T(8,128)(2,1)}, u32[]{:S(2)}) copy-start(bf16[24,512]{1,0:T(8,128)(2,1)} %param.26) | copy-start | bytes 73732
  65.6 18.5 %copy-start.14 = (f32[2048]{0:T(1024)S(1)}, f32[2048]{0:T(1024)}, u32[]{:S(2)}) copy-start(f32[2048]{0:T(1024)} %convert_element_type.149) | copy-start | bytes 24580
  76.6 7.5 %copy-start.7 = (bf16[24,512]{1,0:T(8,128)(2,1)}, bf16[24,512]{1,0:T(8,128)(2,1)S(1)}, u32[]{:S(2)}) copy-start(bf16[24,512]{1,0:T(8,128)(2,1)S(1)} %fusion.28) | copy-start | bytes 73732
  84.2 0.6 copy-start.4
  114.0 0.9 copy-start.3
  117.9 4.2 %copy-start.5 = (bf16[24,2048]{1,0:T(8,128)(2,1)S(1)}, bf16[24,2048]{1,0:T(8,128)(2,1)}, u32[]{:S(2)}) copy-start(bf16[24,2048]{1,0:T(8,128)(2,1)} %copy-done.4) | copy-start | bytes 294916
  117.9 4.2 %copy-start.6 = (bf16[2048,128]{1,0:T(8,128)(2,1)S(1)}, bf16[2048,128]{1,0:T(8,128)(2,1)}, u32[]{:S(2)}) copy-start(bf16[2048,128]{1,0:T(8,128)(2,1)} %param.48) | copy-start | bytes 1572868
  121.8 51.3 %reduce-scatter.5.cloned.1.call-start = ((), (), s32[]{:S(2)}) async-start(), calls=%async_computation.5 | async-start | bytes 122880 | tf_op jit(solution)/shard_map/reduce_scatter | solution.py:121
  144.5 6.3 %copy-start.9 = (f32[24,512]{1,0:T(8,128)S(1)}, f32[24,512]{1,0:T(8,128)}, u32[]{:S(2)}) copy-start(f32[24,512]{1,0:T(8,128)} %get-tuple-element.6) | copy-start | bytes 147460
  144.5 6.3 %copy-start.11 = (f32[24,512]{1,0:T(8,128)S(1)}, f32[24,512]{1,0:T(8,128)}, u32[]{:S(2)}) copy-start(f32[24,512]{1,0:T(8,128)} %copy-done.10) | copy-start | bytes 147460
  150.8 10.4 %copy-start.19 = (f32[96]{0:T(128)S(1)}, f32[96]{0:T(128)}, u32[]{:S(2)}) copy-start(f32[96]{0:T(128)} %copy-done.18) | copy-start | bytes 1156
  150.8 22.3 %copy-start.8 = (bf16[24,512]{1,0:T(8,128)(2,1)S(1)}, bf16[24,512]{1,0:T(8,128)(2,1)}, u32[]{:S(2)}) copy-start(bf16[24,512]{1,0:T(8,128)(2,1)} %copy-done.7) | copy-start | bytes 73732
  157.8 11.6 %all-to-all-start.1 = ((bf16[8,1,18,512]{3,2,1,0:T(8,128)(2,1)}), bf16[8,1,18,512]{3,2,1,0:T(8,128)(2,1)S(1)}, u32[]{:S(2)}, u32[]{:S(2)}) async-start(bf16[8,1,18,512]{3,2,1,0:T(8,128)(2,1)} %bitcast.114), calls=%async_computation.2 | async-start | bytes 393216 | tf_op jit(solution)/shard_map/all_to_all | solution.py:165
Sparse Core Ops, SparseCore 0:
  121.9 24.2 reduce-scatter.2
  149.0 24.0 reduce-scatter.4
where the time goes:
time: 183 us; the launch traced here: 181 us
  blocking collectives  66.8 us (37%)
  local copies, waits for them, and re-layouts  37.1 us (20%)
  other arithmetic  26.2 us (14%)
  matrix products  22.4 us (12%)
  between operations  14.4 us (8%)
  waiting for transfers between devices  10.8 us (6%)
  starting transfers between devices  3.65 us (2%)
    all_to_all x1, blocking collectives, local(): lax.all_to_all(outgoing, 'ep', split_axis=0, concat_axis=0, tiled=True)  25.8 us
    dot_general x12, matrix products, product(): return jnp.dot(left, right, preferred_element_type=jnp.float32)  15.4 us
    psum x1, blocking collectives, local(): lax.psum((product(first_own, decay_down), product(first_own, iclr_down)),...  15.2 us
    mul x2, local copies, waits for them, and re-layouts, local(): recall[..., None] * scaled_removal[:, None]  11.6 us
    mul x3, local copies, waits for them, and re-layouts, local(): value_cols[..., None] * written[:, None]  10.1 us
    all_gather x1, blocking collectives, first_norm_rows(): gathered = lax.all_gather(token_rows, 'tp', axis=1, tiled=True)  10 us
    all_gather x1, blocking collectives, local(): heads_all = lax.all_gather(head_out, 'tp', axis=1, tiled=True)  8.39 us
    all_to_all x1, waiting for transfers between devices, local(): lax.all_to_all(summed, 'ep', split_axis=0, concat_axis=0, tiled=True)  8.19 us
  transfers between devices with their start and end apart: 3, of which 2 were waited for; matrix products, arithmetic and copies ran while one was open for 20% of the time, Pallas kernels for 0%

commit v1 on v0

--- a/solution.py
+++ b/solution.py
@@ -22,7 +22,13 @@
 def first_norm_rows(token_rows, gain):
     own_width = token_rows.shape[1]
     start = lax.axis_index("tp") * own_width
-    gathered = lax.all_gather(token_rows, "tp", axis=1, tiled=True)
+    size = lax.axis_size("tp")
+    held, parts = (token_rows, [token_rows])
+    for _ in range(size - 1):
+        held = lax.ppermute(held, "tp", [(i, (i + 1) % size) for i in range(size)])
+        parts.insert(0, held)
+    line = jnp.concatenate(parts, axis=1)
+    gathered = jnp.roll(line, (lax.axis_index("tp") + 1) * token_rows.shape[1], axis=1)
     values = gathered.astype(jnp.float32)
     full_rows = scale_rows(values, jnp.mean(values * values, axis=1, keepdims=True), gain)
     own_cols = lax.dynamic_slice_in_dim(full_rows, start, own_width, 1)

time: 183 us -> 184 us (level)
  blocking collectives: 66.8 us -> 33.2 us
  waiting for transfers between devices: 10.8 us -> 40.7 us
  starting transfers between devices: 3.65 us -> 13.6 us
  matrix products: 22.4 us -> 19.3 us
    all_to_all x1 -> x0, blocking collectives: 25.8 us -> none  [local(): lax.all_to_all(outgoing, 'ep', split_axis=0, concat_axis=0, tiled=True)]
    all_to_all x0 -> x1, waiting for transfers between devices: none -> 21 us  [local(): lax.all_to_all(outgoing, 'ep', split_axis=0, concat_axis=0, tiled=True)]
    reduce_scatter x1, waiting for transfers between devices: 2.57 us -> 12.9 us  [local(): lax.psum_scatter(product(dense_hidden, dense_down).astype(jnp.bfloat16),...]
    all_gather x1 -> x0, blocking collectives: 10 us -> none  [first_norm_rows(): gathered = lax.all_gather(token_rows, 'tp', axis=1, tiled=True)]
    all_to_all x1, waiting for transfers between devices: 8.19 us -> 1.14 us  [local(): lax.all_to_all(summed, 'ep', split_axis=0, concat_axis=0, tiled=True)]
    ppermute x0 -> x3, waiting for transfers between devices: none -> 5.64 us  [first_norm_rows(): held = lax.ppermute(held, 'tp', [(i, (i + 1) % size) for i in range(size)])]
    all_to_all x0 -> x1, starting transfers between devices: none -> 4.88 us  [local(): lax.all_to_all(outgoing, 'ep', split_axis=0, concat_axis=0, tiled=True)]
    ppermute x0 -> x3, starting transfers between devices: none -> 4.33 us  [first_norm_rows(): held = lax.ppermute(held, 'tp', [(i, (i + 1) % size) for i in range(size)])]
  transfers between devices with their start and end apart: 3 -> 7, of which waited for: 2 -> 5; matrix products, arithmetic and copies ran while one was open for 20% -> 24% of each run, Pallas kernels for 0% -> 0%
where the time goes in v1:
time: 184 us; the launch traced here: 183 us
  waiting for transfers between devices  40.7 us (22%)
  local copies, waits for them, and re-layouts  35.5 us (19%)
  blocking collectives  33.2 us (18%)
  other arithmetic  26 us (14%)
  matrix products  19.3 us (10%)
  between operations  14.6 us (8%)
  starting transfers between devices  13.6 us (7%)
    all_to_all x1, waiting for transfers between devices, local(): lax.all_to_all(outgoing, 'ep', split_axis=0, concat_axis=0, tiled=True)  21 us
    psum x1, blocking collectives, local(): lax.psum((product(first_own, decay_down), product(first_own, iclr_down)),...  17.1 us
    reduce_scatter x1, waiting for transfers between devices, local(): lax.psum_scatter(product(dense_hidden, dense_down).astype(jnp.bfloat16),...  12.9 us
    dot_general x12, matrix products, product(): return jnp.dot(left, right, preferred_element_type=jnp.float32)  12.9 us
    mul x2, local copies, waits for them, and re-layouts, local(): recall[..., None] * scaled_removal[:, None]  11.4 us
    mul x3, local copies, waits for them, and re-layouts, local(): value_cols[..., None] * written[:, None]  10.2 us
    reduce_sum x1, other arithmetic, local(): jnp.sum(state_grid * recept.astype(jnp.float32).reshape(seq_count, 1, hea...  8.51 us
    all_gather x1, blocking collectives, local(): heads_all = lax.all_gather(head_out, 'tp', axis=1, tiled=True)  8.26 us
  transfers between devices with their start and end apart: 7, of which 5 were waited for; matrix products, arithmetic and copies ran while one was open for 24% of the time, Pallas kernels for 0%

profile of v1, /device:TPU:0, one launch (start us, length us, event | category | flops | bytes accessed | tf_op | source)
XLA Modules:
  0.0 182.7 jit_solution(7930463979639800963)
XLA Ops:
  7.2 3.0 %collective-permute-start = (bf16[24,512]{1,0:T(8,128)(2,1)}, bf16[24,512]{1,0:T(8,128)(2,1)S(1)}, u32[]{:S(2)}, u32[]{:S(2)}) collective-permute-start(bf16[24,512]{1,0:T(8,128)(2,1)} %param.26), channel_id=1, source_target_pairs={{0,1},{1,2},{2,3},{3,0},{4,5},{5,6},{6,7},{7,4},{8,9},{9,10},{10,1... | collective-permute-start | bytes 73736 | tf_op jit(solution)/shard_map/ppermute | solution.py:28
  11.1 2.1 %collective-permute-done = bf16[24,512]{1,0:T(8,128)(2,1)S(1)} collective-permute-done((bf16[24,512]{1,0:T(8,128)(2,1)}, bf16[24,512]{1,0:T(8,128)(2,1)S(1)}, u32[]{:S(2)}, u32[]{:S(2)}) %collective-permute-start) | collective-permute-done | bytes 24608 | tf_op jit(solution)/shard_map/ppermute | solution.py:28
  13.2 1.1 collective-permute-start.1
  14.4 3.5 %collective-permute-done.1 = bf16[24,512]{1,0:T(8,128)(2,1)S(1)} collective-permute-done((bf16[24,512]{1,0:T(8,128)(2,1)S(1)}, bf16[24,512]{1,0:T(8,128)(2,1)S(1)}, u32[]{:S(2)}, u32[]{:S(2)}) %collective-permute-start.1) | collective-permute-done | bytes 24608 | tf_op jit(solution)/shard_map/ppermute | solution.py:28
  22.9 5.6 %reshape.195 = f32[24,64,8,64]{3,2,1,0:T(8,128)} reshape(f32[24,64,512]{2,1,0:T(8,128)} %param.27) | data formatting | bytes 6291456 | tf_op jit(solution)/shard_map/reshape | solution.py:97
  29.2 2.0 %fusion.29 = f32[24,512]{1,0:T(8,128)S(1)} fusion(bf16[24,2048]{1,0:T(8,128)(2,1)S(1)} %fusion.51, bf16[2048,512]{1,0:T(8,128)(2,1)} %param.29), kind=kOutput, calls=%fused_computation.30 | convolution fusion | flops 50356224 | bytes 2244608 | tf_op jit(solution)/shard_map/dot_general | solution.py:13
  31.3 2.0 %fusion.30 = f32[24,512]{1,0:T(8,128)S(1)} fusion(bf16[24,2048]{1,0:T(8,128)(2,1)S(1)} %fusion.51, bf16[2048,512]{1,0:T(8,128)(2,1)} %param.31), kind=kOutput, calls=%fused_computation.32 | convolution fusion | flops 50356224 | bytes 2244608 | tf_op jit(solution)/shard_map/dot_general | solution.py:13
  33.4 2.0 %broadcast_multiply_fusion.1 = (f32[24,512]{1,0:T(8,128)S(1)}, f32[24,512]{1,0:T(8,128)S(1)}) fusion(f32[512]{0:T(512)S(1)} %convert_element_type.135, bf16[24,2048]{1,0:T(8,128)(2,1)S(1)} %fusion.51, bf16[2048,512]{1,0:T(8,128)(2,1)} %param.30), kind=kOutput, calls=%fused_computation.81 | convolution fusion | flops 50368512 | bytes 2295808 | tf_op jit(solution)/shard_map/dot_general | solution.py:13
  35.7 17.1 %all-reduce = (bf16[24,96]{1,0:T(8,128)(2,1)S(1)}, f32[24,96]{1,0:T(8,128)S(1)}) all-reduce(f32[24,96]{1,0:T(8,128)S(1)} %fusion.62, f32[24,96]{1,0:T(8,128)S(1)} %fusion.64), channel_id=1, replica_groups=mesh['ep'=8,'tp'=4] {'tp'}, use_global_device_ids=true, to_apply=%region_4.5 | all-reduce | flops 4608 | bytes 32256 | tf_op jit(solution)/shard_map/psum | solution.py:79
  52.8 0.8 multiply_multiply_fusion
  55.0 4.5 %multiply_reduce_fusion.1 = f32[24,64,8]{2,1,0:T(8,128)S(1)} fusion(f32[24,64,8,64]{3,2,1,0:T(8,128)} %reshape.195, f32[24,8,64]{2,1,0:T(8,128)S(1)} %get-tuple-element.5), kind=kLoop, calls=%fused_computation.2 | loop fusion | flops 1560576 | bytes 3244032 | tf_op jit(solution)/shard_map/reduce_sum | solution.py:98
  59.5 8.5 %multiply_reduce_fusion = f32[24,64,8]{2,1,0:T(8,128)S(1)} fusion(f32[24,64,8,64]{3,2,1,0:T(8,128)} %reshape.195, f32[24,8,64]{2,1,0:T(8,128)S(1)} %reshape.208, f32[24,8,64]{2,1,0:T(8,128)S(1)} %mul.284, f32[24,64,8]{2,1,0:T(8,128)S(1)} %copy.44, f32[24,8,64]{2,1,0:T(8,128)S(1)} %get-tuple-element.4, f32[24,64,8]{2,1,0:T(8,128)S(1)} %multiply_reduce_fusion.1, ...), kind=kLoop, calls=%fused_computation.1 | loop fusion | flops 5492736 | bytes 3489792 | tf_op jit(solution)/shard_map/reduce_sum | solution.py:108
  68.7 8.3 %all_gather.6 = bf16[24,2048]{1,0:T(8,128)(2,1)S(1)} all-gather(bf16[24,512]{1,0:T(8,128)(2,1)S(1)} %convert_element_type.141), channel_id=1, replica_groups=mesh['ep'=8,'tp'=4] {'tp'}, dimensions={1}, use_global_device_ids=true | all-gather | bytes 122880 | tf_op jit(solution)/shard_map/all_gather | solution.py:120
  77.0 2.0 %fusion.28 = bf16[24,512]{1,0:T(8,128)(2,1)S(1)} fusion(bf16[24,2048]{1,0:T(8,128)(2,1)S(1)} %all_gather.6, bf16[2048,512]{1,0:T(8,128)(2,1)} %param.41, bf16[24,512]{1,0:T(8,128)(2,1)S(1)} %copy-done.6), kind=kOutput, calls=%fused_computation.28 | convolution fusion | flops 50393088 | bytes 2244608 | tf_op jit(solution)/shard_map/dot_general | solution.py:13
  79.0 7.8 %all_gather.7 = bf16[24,2048]{1,0:T(8,128)(2,1)S(1)} all-gather(bf16[24,512]{1,0:T(8,128)(2,1)S(1)} %fusion.28), channel_id=1, replica_groups=mesh['ep'=8,'tp'=4] {'tp'}, dimensions={1}, use_global_device_ids=true | all-gather | bytes 122880 | tf_op jit(solution)/shard_map/all_gather | solution.py:41
  87.9 0.8 reshape.200
  88.7 1.3 convolution_convert_fusion.1
  90.0 1.1 reshape.201
  91.1 4.9 %all-to-all-start = ((bf16[8,1,18,2048]{3,2,1,0:T(8,128)(2,1)}), bf16[8,1,18,2048]{3,2,1,0:T(8,128)(2,1)}, u32[]{:S(2)}, u32[]{:S(2)}) async-start(bf16[8,1,18,2048]{3,2,1,0:T(8,128)(2,1)} %bitcast.112), calls=%async_computation | async-start | bytes 1572864 | tf_op jit(solution)/shard_map/all_to_all | solution.py:157
  96.1 21.0 %all-to-all-done = bf16[8,1,18,2048]{3,2,1,0:T(8,128)(2,1)} async-done(((bf16[8,1,18,2048]{3,2,1,0:T(8,128)(2,1)}), bf16[8,1,18,2048]{3,2,1,0:T(8,128)(2,1)}, u32[]{:S(2)}, u32[]{:S(2)}) %all-to-all-start) | async-done | bytes 589856 | tf_op jit(solution)/shard_map/all_to_all | solution.py:157
  117.0 2.4 %fusion.6 = f32[8,1,18,512]{3,2,0,1:T(8,128)S(1)} fusion(bf16[1,2048,512]{2,1,0:T(8,128)(2,1)} %param.45, bf16[8,1,18,2048]{3,2,1,0:T(8,128)(2,1)} %all-to-all-done), kind=kOutput, calls=%fused_computation.13 | convolution fusion | flops 301989888 | bytes 2981888 | tf_op jit(solution)/shard_map/secd,edf->secf/dot_general | solution.py:158
  119.5 3.8 %fusion = bf16[8,1,18,2048]{3,2,0,1:T(8,128)(2,1)} fusion(bf16[1,512,2048]{2,1,0:T(8,128)(2,1)S(1)} %copy-done, bf16[1,2048,512]{2,1,0:T(8,128)(2,1)} %param.46, bf16[8,1,18,2048]{3,2,1,0:T(8,128)(2,1)} %all-to-all-done, f32[8,1,18,512]{3,2,0,1:T(8,128)S(1)} %fusion.6), kind=kOutput, calls=%fused_computation.6 | convolution fusion | flops 604717056 | bytes 5668864 | tf_op jit(solution)/shard_map/secf,efd->secd/dot_general | solution.py:161
  124.0 5.1 %mul.276 = f32[24,64,8,64]{3,2,1,0:T(8,128)} broadcast(f32[24,64,8]{2,1,0:T(8,128)} %copy-done.1), dimensions={0,1,2} | broadcast | bytes 3194880 | tf_op jit(solution)/shard_map/mul | solution.py:105
  129.1 6.3 %mul.319 = f32[24,64,512]{2,1,0:T(8,128)} reshape(f32[24,64,8,64]{3,2,1,0:T(8,128)} %mul.276) | data formatting | bytes 6291456 | tf_op jit(solution)/shard_map/mul | solution.py:105
  135.4 3.8 %mul.280 = f32[24,64,8,64]{3,2,1,0:T(8,128)} broadcast(f32[24,64,8]{2,1,0:T(8,128)S(1)} %copy.44), dimensions={0,1,2} | broadcast | bytes 3194880 | tf_op jit(solution)/shard_map/mul | solution.py:106
  139.2 6.4 %mul.325 = f32[24,64,512]{2,1,0:T(8,128)} reshape(f32[24,64,8,64]{3,2,1,0:T(8,128)} %mul.280) | data formatting | bytes 6291456 | tf_op jit(solution)/shard_map/mul | solution.py:106
  145.8 2.0 %convolution_convert_fusion.2 = bf16[24,2048]{1,0:T(8,128)(2,1)} fusion(bf16[128,2048]{1,0:T(8,128)(2,1)S(1)} %copy-done.5, bf16[24,2048]{1,0:T(8,128)(2,1)S(1)} %copy-done.3, bf16[2048,128]{1,0:T(8,128)(2,1)} %param.49, f32[24,128]{1,0:T(8,128)S(1)} %fusion.80), kind=kOutput, calls=%fused_computation.7 | convolution fusion | flops 25233408 | bytes 1257472 | tf_op jit(solution)/shard_map/dot_general | solution.py:13
  147.9 4.3 %all-to-all-start.1 = ((bf16[8,1,18,512]{3,2,1,0:T(8,128)(2,1)}), bf16[8,1,18,512]{3,2,1,0:T(8,128)(2,1)S(1)}, u32[]{:S(2)}, u32[]{:S(2)}) async-start(bf16[8,1,18,512]{3,2,1,0:T(8,128)(2,1)} %bitcast.114), calls=%async_computation.2 | async-start | bytes 393216 | tf_op jit(solution)/shard_map/all_to_all | solution.py:171
  152.2 7.0 %multiply_add_fusion = f32[24,64,512]{2,1,0:T(8,128)} fusion(f32[24,64,512]{2,1,0:T(8,128)} %mul.325, f32[24,64,512]{2,1,0:T(8,128)} %mul.319, f32[24,64,512]{2,1,0:T(8,128)} %param.27, f32[24,512]{1,0:T(8,128)S(1)} %get-tuple-element.7, f32[24,512]{1,0:T(8,128)S(1)} %copy-done.9, f32[24,512]{1,0:T(8,128)S(1)} %copy-done.11), kind=kLoop, calls=%fused_computation.3 | loop fusion | flops 3932160 | bytes 12730368 | tf_op jit(solution)/shard_map/add | solution.py:104
  159.4 1.1 all-to-all-done.1
  161.6 12.9 %reduce-scatter.5.cloned.1.call-done = bf16[24,512]{1,0:T(8,128)(2,1)} async-done(((bf16[24,2048]{1,0:T(8,128)(2,1)}), bf16[24,512]{1,0:T(8,128)(2,1)}) %reduce-scatter.5.cloned.1.call-update) | async-done | bytes 24592 | tf_op jit(solution)/shard_map/reduce_scatter | solution.py:127
  174.5 1.4 add_convert_fusion
  (120 shorter events, 12.3 us)
Async XLA Ops:
  7.2 112.3 %copy-start = (bf16[1,512,2048]{2,1,0:T(8,128)(2,1)S(1)}, bf16[1,512,2048]{2,1,0:T(8,128)(2,1)}, u32[]{:S(2)}) copy-start(bf16[1,512,2048]{2,1,0:T(8,128)(2,1)} %param.47) | copy-start | bytes 6291460
  7.2 6.0 %collective-permute-start = (bf16[24,512]{1,0:T(8,128)(2,1)}, bf16[24,512]{1,0:T(8,128)(2,1)S(1)}, u32[]{:S(2)}, u32[]{:S(2)}) collective-permute-start(bf16[24,512]{1,0:T(8,128)(2,1)} %param.26), channel_id=1, source_target_pairs={{0,1},{1,2},{2,3},{3,0},{4,5},{5,6},{6,7},{7,4},{8,9},{9,10},{10,1... | collective-permute-start | bytes 73736 | tf_op jit(solution)/shard_map/ppermute | solution.py:28
  13.2 4.7 %collective-permute-start.1 = (bf16[24,512]{1,0:T(8,128)(2,1)S(1)}, bf16[24,512]{1,0:T(8,128)(2,1)S(1)}, u32[]{:S(2)}, u32[]{:S(2)}) collective-permute-start(bf16[24,512]{1,0:T(8,128)(2,1)S(1)} %collective-permute-done), channel_id=1, source_target_pairs={{0,1},{1,2},{2,3},{3,0},{4,5},{5,6},{6,7},{7,4},{8,9},{9,10},{10,1... | collective-permute-start | bytes 73736 | tf_op jit(solution)/shard_map/ppermute | solution.py:28
  14.4 4.3 %copy-start.22 = (f32[96]{0:T(128)}, f32[96]{0:T(128)S(1)}, u32[]{:S(2)}) copy-start(f32[96]{0:T(128)S(1)} %fusion.33) | copy-start | bytes 1156
  17.9 10.6 %collective-permute-start.2 = (bf16[24,512]{1,0:T(8,128)(2,1)S(1)}, bf16[24,512]{1,0:T(8,128)(2,1)S(1)}, u32[]{:S(2)}, u32[]{:S(2)}) collective-permute-start(bf16[24,512]{1,0:T(8,128)(2,1)S(1)} %collective-permute-done.1), channel_id=1, source_target_pairs={{0,1},{1,2},{2,3},{3,0},{4,5},{5,6},{6,7},{7,4},{8,9},{9,10},{10,1... | collective-permute-start | bytes 73736 | tf_op jit(solution)/shard_map/ppermute | solution.py:28
  22.9 5.7 %copy-start.6 = (bf16[24,512]{1,0:T(8,128)(2,1)S(1)}, bf16[24,512]{1,0:T(8,128)(2,1)}, u32[]{:S(2)}) copy-start(bf16[24,512]{1,0:T(8,128)(2,1)} %param.26) | copy-start | bytes 73732
  22.9 6.0 %copy-start.13 = (bf16[512,96]{0,1:T(8,128)(2,1)S(1)}, bf16[512,96]{0,1:T(8,128)(2,1)}, u32[]{:S(2)}) copy-start(bf16[512,96]{0,1:T(8,128)(2,1)} %param.35) | copy-start | bytes 294916
  22.9 6.1 %copy-start.14 = (bf16[512,96]{0,1:T(8,128)(2,1)S(1)}, bf16[512,96]{0,1:T(8,128)(2,1)}, u32[]{:S(2)}) copy-start(bf16[512,96]{0,1:T(8,128)(2,1)} %param.32) | copy-start | bytes 294916
  31.1 21.7 %copy-start.15 = (bf16[96,512]{1,0:T(8,128)(2,1)S(1)}, bf16[96,512]{1,0:T(8,128)(2,1)}, u32[]{:S(2)}) copy-start(bf16[96,512]{1,0:T(8,128)(2,1)} %param.36) | copy-start | bytes 294916
  31.1 21.7 %copy-start.18 = (f32[512]{0:T(512)S(1)}, f32[512]{0:T(512)}, u32[]{:S(2)}) copy-start(f32[512]{0:T(512)} %param.37) | copy-start | bytes 6148
  31.2 22.6 %copy-start.20 = (bf16[96,512]{1,0:T(8,128)(2,1)S(1)}, bf16[96,512]{1,0:T(8,128)(2,1)}, u32[]{:S(2)}) copy-start(bf16[96,512]{1,0:T(8,128)(2,1)} %param.33) | copy-start | bytes 294916
  31.3 22.6 %copy-start.21 = (f32[512]{0:T(512)S(1)}, f32[512]{0:T(512)}, u32[]{:S(2)}) copy-start(f32[512]{0:T(512)} %param.34) | copy-start | bytes 6148
  54.1 0.6 copy-start.10
  59.5 8.5 %copy-start.1 = (f32[24,64,8]{2,1,0:T(8,128)}, f32[24,64,8]{2,1,0:T(8,128)S(1)}, u32[]{:S(2)}) copy-start(f32[24,64,8]{2,1,0:T(8,128)S(1)} %multiply_reduce_fusion.1) | copy-start | bytes 147460
  59.5 8.8 %copy-start.12 = (f32[8,64]{0,1:T(8,128)S(1)}, f32[8,64]{0,1:T(8,128)}, u32[]{:S(2)}) copy-start(f32[8,64]{0,1:T(8,128)} %copy.45) | copy-start | bytes 6148
  79.0 8.0 %copy-start.7 = (bf16[24,512]{1,0:T(8,128)(2,1)}, bf16[24,512]{1,0:T(8,128)(2,1)S(1)}, u32[]{:S(2)}) copy-start(bf16[24,512]{1,0:T(8,128)(2,1)S(1)} %fusion.28) | copy-start | bytes 73732
  79.0 17.0 %copy-start.23 = (f32[96]{0:T(128)S(1)}, f32[96]{0:T(128)}, u32[]{:S(2)}) copy-start(f32[96]{0:T(128)} %copy-done.22) | copy-start | bytes 1156
  79.0 17.1 %copy-start.17 = (bf16[2048]{0:T(1024)(128)(2,1)S(1)}, bf16[2048]{0:T(1024)(128)(2,1)}, u32[]{:S(2)}) copy-start(bf16[2048]{0:T(1024)(128)(2,1)} %param.51) | copy-start | bytes 12292
  87.1 0.6 copy-start.2
  91.1 25.9 %all-to-all-start = ((bf16[8,1,18,2048]{3,2,1,0:T(8,128)(2,1)}), bf16[8,1,18,2048]{3,2,1,0:T(8,128)(2,1)}, u32[]{:S(2)}, u32[]{:S(2)}) async-start(bf16[8,1,18,2048]{3,2,1,0:T(8,128)(2,1)} %bitcast.112), calls=%async_computation | async-start | bytes 1572864 | tf_op jit(solution)/shard_map/all_to_all | solution.py:157
  96.0 51.9 %reduce-scatter.3.cloned.1.call-start = ((), (), s32[]{:S(2)}) async-start(), calls=%async_computation.4 | async-start | bytes 983040 | tf_op jit(solution)/shard_map/reduce_scatter | solution.py:165
  119.5 3.9 %copy-start.16 = (s32[24,4]{0,1:T(4,128)S(1)}, s32[24,4]{0,1:T(4,128)}, u32[]{:S(2)}) copy-start(s32[24,4]{0,1:T(4,128)} %param.43) | copy-start | bytes 1156
  119.5 4.1 %copy-start.19 = (f32[24,4]{0,1:T(4,128)S(1)}, f32[24,4]{0,1:T(4,128)}, u32[]{:S(2)}) copy-start(f32[24,4]{0,1:T(4,128)} %param.44) | copy-start | bytes 1156
  123.3 51.1 %reduce-scatter.5.cloned.1.call-start = ((), (), s32[]{:S(2)}) async-start(), calls=%async_computation.5 | async-start | bytes 122880 | tf_op jit(solution)/shard_map/reduce_scatter | solution.py:127
  139.2 6.4 %copy-start.3 = (bf16[24,2048]{1,0:T(8,128)(2,1)S(1)}, bf16[24,2048]{1,0:T(8,128)(2,1)}, u32[]{:S(2)}) copy-start(bf16[24,2048]{1,0:T(8,128)(2,1)} %copy-done.2) | copy-start | bytes 294916
  139.2 6.4 %copy-start.4 = (bf16[2048,128]{1,0:T(8,128)(2,1)S(1)}, bf16[2048,128]{1,0:T(8,128)(2,1)}, u32[]{:S(2)}) copy-start(bf16[2048,128]{1,0:T(8,128)(2,1)} %param.48) | copy-start | bytes 1572868
  139.2 6.6 %copy-start.5 = (bf16[128,2048]{1,0:T(8,128)(2,1)S(1)}, bf16[128,2048]{1,0:T(8,128)(2,1)}, u32[]{:S(2)}) copy-start(bf16[128,2048]{1,0:T(8,128)(2,1)} %param.50) | copy-start | bytes 1572868
  139.2 13.0 %copy-start.9 = (f32[24,512]{1,0:T(8,128)S(1)}, f32[24,512]{1,0:T(8,128)}, u32[]{:S(2)}) copy-start(f32[24,512]{1,0:T(8,128)} %get-tuple-element.6) | copy-start | bytes 147460
  139.2 13.0 %copy-start.11 = (f32[24,512]{1,0:T(8,128)S(1)}, f32[24,512]{1,0:T(8,128)}, u32[]{:S(2)}) copy-start(f32[24,512]{1,0:T(8,128)} %copy-done.10) | copy-start | bytes 147460
  147.9 12.6 %all-to-all-start.1 = ((bf16[8,1,18,512]{3,2,1,0:T(8,128)(2,1)}), bf16[8,1,18,512]{3,2,1,0:T(8,128)(2,1)S(1)}, u32[]{:S(2)}, u32[]{:S(2)}) async-start(bf16[8,1,18,512]{3,2,1,0:T(8,128)(2,1)} %bitcast.114), calls=%async_computation.2 | async-start | bytes 393216 | tf_op jit(solution)/shard_map/all_to_all | solution.py:171
  152.2 22.3 %copy-start.8 = (bf16[24,512]{1,0:T(8,128)(2,1)S(1)}, bf16[24,512]{1,0:T(8,128)(2,1)}, u32[]{:S(2)}) copy-start(bf16[24,512]{1,0:T(8,128)(2,1)} %copy-done.7) | copy-start | bytes 73732
Sparse Core Ops, SparseCore 0:
  123.5 24.0 reduce-scatter.2
  150.3 24.0 reduce-scatter.4
